TPU v7x, 32 devices: a whole 2x2x4 slice. The times are simulated.
32 devices in a mesh: ep: 8 (over z, x), tp: 4 (over y, core).
Axes of the slice: x: 2, y: 2, z: 4, core: 2. Of those that a mesh axis runs over, the one named last changes fastest.
Arguments:
- tokens: bfloat16 [128, 4096], P('ep'), may hold values from -6 to 6
- norm_gain: float32 [4096], replicated, may hold values from 0.1 to 1.9
- query_weight: bfloat16 [4096, 2048], P('ep', 'tp'), may hold values from -0.09375 to 0.09375
- key_weight: bfloat16 [4096, 256], P('ep', 'tp'), may hold values from -0.09375 to 0.09375
- value_weight: bfloat16 [4096, 256], P('ep', 'tp'), may hold values from -0.09375 to 0.09375
- forget_weight: bfloat16 [4096, 32], P('ep', 'tp'), may hold values from -0.09375 to 0.09375
- forget_bias: float32 [32], P('tp'), may hold values from -1 to 2
- kv_cache: bfloat16 [128, 1024, 4, 128], P('ep', None, 'tp'), may hold values from -256 to 256, as said below
- log_gates: float32 [128, 1024, 32], P('ep', None, 'tp'), may hold values from -258 to 0
- lengths: int32 [128], P('ep'), may hold values from 128 to 1024, as said below
- out_weight: bfloat16 [2048, 4096], P('tp', 'ep'), may hold values from -0.125 to 0.125
- mix_gain: float32 [4096], replicated, may hold values from 0.1 to 1.9
- expert_gate: bfloat16 [8, 4096, 1024], P('ep', None, 'tp'), may hold values from -0.09375 to 0.09375
- expert_up: bfloat16 [8, 4096, 1024], P('ep', None, 'tp'), may hold values from -0.09375 to 0.09375
- expert_down: bfloat16 [8, 1024, 4096], P('ep', 'tp'), may hold values from -0.1875 to 0.1875
- routes: int32 [128, 4], P('ep'), may hold values from 0 to 7, all different within a row; in each aligned block of 16 rows (0 to 15, 16 to 31, ...) at most 16 rows name the same one
- route_weights: float32 [128, 4], P('ep'), may hold values from 0.2 to 1
- dense_gate: bfloat16 [4096, 4096], P(None, 'ep'), may hold values from -0.09375 to 0.09375
- dense_up: bfloat16 [4096, 4096], P(None, 'ep'), may hold values from -0.09375 to 0.09375
- dense_down: bfloat16 [4096, 4096], P('ep', 'tp'), may hold values from -0.09375 to 0.09375
- gate_vector: float32 [4096], replicated, may hold values from -0.09375 to 0.09375
Outputs:
- layer_out: bfloat16 [128, 4096], P('ep', 'tp')
Inputs may be any that keep to these rules, and one draw needn't show every extreme that they name: `kv_cache`: keys and values of the cached positions. `lengths`: some sequence uses all 1024 cached positions in every draw. A sequence's 4 experts differ. Among the routes of the 16 sequences of one index of ep no expert appears more than 16 times, and in every draw some expert appears exactly 16 times there; every expert is chosen somewhere.
All inputs are finite; a program needn't handle non-finite values.
Results may differ from a plain program's by a relative error of at most 0.012.
The roundings to bfloat16 on the way count: a program that leaves them out, or rounds other values in their place, can miss the bound.
Values may be sent and summed in bfloat16 or wider, within the bound.
No kernel may reach another device: no remote copies, remote signals or barrier semaphores. Data moves between devices by JAX's collectives and lax.ppermute only.
A program may use at most 128 MiB of HBM per device.

v0:
```python
import jax
import jax.numpy as jnp
from jax import lax
from jax.sharding import PartitionSpec as P

EPS = 1e-06


def rms_scaled(matrix, gains):
    values = matrix.astype(jnp.float32)
    return values * lax.rsqrt(jnp.mean(values * values, axis=-1, keepdims=True) + EPS) * gains


def attend_local(queries, key_new, value_new, forget, kv_cache, log_gates, lengths):
    seqs_here, cache_len, kv_count, double_width = kv_cache.shape
    head_width = double_width // 2
    group_size = queries.shape[1] // (kv_count * head_width)
    queries = queries.reshape(seqs_here, kv_count, group_size, head_width)
    key_new = key_new.reshape(seqs_here, kv_count, head_width)
    value_new = value_new.reshape(seqs_here, kv_count, head_width)
    cached_keys = kv_cache[..., :head_width]
    cached_values = kv_cache[..., head_width:]
    score_scale = head_width ** (-0.5)
    current_position = jnp.arange(cache_len, dtype=jnp.int32)
    is_last = (current_position[None, :] == lengths[:, None] - 1)[:, :, None]
    last_gate = jnp.sum(jnp.where(is_last, log_gates, 0.0), axis=1)
    newest = last_gate + forget
    gate_bias = newest[:, None, :] - log_gates
    gate_bias = gate_bias.reshape(seqs_here, cache_len, kv_count, group_size).transpose(0, 2, 3, 1)
    past_scores = (
        jnp.einsum("skgd,slkd->skgl", queries, cached_keys, preferred_element_type=jnp.float32)
        * score_scale
        + gate_bias
    )
    is_valid = (current_position[None, :] < lengths[:, None])[:, None, None, :]
    past_scores = jnp.where(is_valid, past_scores, -jnp.inf)
    own_score = (
        jnp.einsum("skgd,skd->skg", queries, key_new, preferred_element_type=jnp.float32)
        * score_scale
    )
    highest = jnp.maximum(jnp.max(past_scores, axis=-1), own_score)
    past_exp = jnp.exp(past_scores - highest[..., None])
    own_exp = jnp.exp(own_score - highest)
    totals = jnp.sum(past_exp, axis=-1) + own_exp
    past_weights = (past_exp / totals[..., None]).astype(jnp.bfloat16)
    own_weights = (own_exp / totals).astype(jnp.bfloat16)
    mixed_values = jnp.einsum(
        "skgl,slkd->skgd", past_weights, cached_values, preferred_element_type=jnp.float32
    )
    mixed_values = (
        mixed_values
        + own_weights.astype(jnp.float32)[..., None] * value_new.astype(jnp.float32)[:, :, None, :]
    )
    return mixed_values.astype(jnp.bfloat16).reshape(seqs_here, kv_count * group_size * head_width)


def shards(
    tokens,
    norm_gain,
    query_weight,
    key_weight,
    value_weight,
    forget_weight,
    forget_bias,
    kv_cache,
    log_gates,
    lengths,
    out_weight,
    mix_gain,
    expert_gate,
    expert_up,
    expert_down,
    routes,
    route_weights,
    dense_gate,
    dense_up,
    dense_down,
    gate_vector,
):
    seq_count = tokens.shape[0]
    normed = rms_scaled(tokens, norm_gain).astype(jnp.bfloat16)
    query_cols = query_weight.shape[1]
    key_cols = key_weight.shape[1]
    columns = lax.all_to_all(normed, "ep", split_axis=1, concat_axis=0, tiled=True)
    row_block = columns
    projected = lax.psum_scatter(
        jnp.concatenate(
            [
                jnp.dot(row_block, matrix, preferred_element_type=jnp.float32)
                for matrix in (query_weight, key_weight, value_weight, forget_weight)
            ],
            axis=1,
        ),
        "ep",
        scatter_dimension=0,
        tiled=True,
    )
    queries = projected[:, :query_cols].astype(jnp.bfloat16)
    key_new = projected[:, query_cols : query_cols + key_cols].astype(jnp.bfloat16)
    value_new = projected[:, query_cols + key_cols : query_cols + 2 * key_cols].astype(jnp.bfloat16)
    forget = jax.nn.log_sigmoid(projected[:, query_cols + 2 * key_cols :] + forget_bias)
    attended = attend_local(queries, key_new, value_new, forget, kv_cache, log_gates, lengths)
    column_terms = jnp.dot(
        lax.all_gather(attended, "ep", axis=0, tiled=True),
        out_weight,
        preferred_element_type=jnp.float32,
    )
    column_total = lax.psum(column_terms, "tp")
    summed = lax.all_to_all(column_total, "ep", split_axis=0, concat_axis=1, tiled=True)
    mixed = (tokens.astype(jnp.float32) + summed).astype(jnp.bfloat16)
    second = rms_scaled(mixed, mix_gain).astype(jnp.bfloat16)
    gate_value = jax.nn.sigmoid(
        jnp.dot(second.astype(jnp.float32), gate_vector, precision=lax.Precision.HIGHEST)
    )
    experts = lax.axis_size("ep")
    top_count = routes.shape[1]
    capacity = max(2, 2 * seq_count * top_count // experts)
    flat_routes = routes.reshape(-1)
    one_hot = (flat_routes[:, None] == jnp.arange(experts, dtype=jnp.int32)[None, :]).astype(
        jnp.int32
    )
    earlier = jnp.sum((jnp.cumsum(one_hot, axis=0) - one_hot) * one_hot, axis=1)
    slot_index = (flat_routes * capacity + earlier).reshape(seq_count, top_count)
    slot_ids = jnp.arange(experts * capacity, dtype=jnp.int32)
    dispatch_map = jnp.any(slot_index[None, :, :] == slot_ids[:, None, None], axis=2).astype(
        jnp.bfloat16
    )
    outgoing = jnp.dot(dispatch_map, second, preferred_element_type=jnp.float32).astype(
        jnp.bfloat16
    )
    outgoing = outgoing.reshape(experts, capacity, second.shape[1])
    received = lax.all_to_all(outgoing, "ep", split_axis=0, concat_axis=0, tiled=True)
    sources, items, model_width = received.shape
    flat_rows = received.reshape(sources * items, model_width)
    gate_pre = jnp.dot(flat_rows, expert_gate[0], preferred_element_type=jnp.float32)
    up_pre = jnp.dot(flat_rows, expert_up[0], preferred_element_type=jnp.float32)
    hidden = (jax.nn.silu(gate_pre) * up_pre).astype(jnp.bfloat16)
    partial_rows = jnp.dot(hidden, expert_down[0], preferred_element_type=jnp.float32)
    reduced = lax.psum_scatter(partial_rows, "tp", scatter_dimension=1, tiled=True)
    replies = reduced.astype(jnp.bfloat16).reshape(sources, items, reduced.shape[1])
    returned = lax.all_to_all(replies, "ep", split_axis=0, concat_axis=0, tiled=True)
    quarter_cols = returned.shape[2]
    picked = returned.reshape(experts * capacity, quarter_cols)[slot_index.reshape(-1)]
    routed = jnp.sum(
        picked.astype(jnp.float32).reshape(seq_count, top_count, quarter_cols)
        * route_weights[:, :, None],
        axis=1,
    )
    tp_index = lax.axis_index("tp")
    piece = lax.all_gather(second, "ep", axis=0, tiled=True)
    dense_hidden = (
        jax.nn.silu(jnp.dot(piece, dense_gate, preferred_element_type=jnp.float32))
        * jnp.dot(piece, dense_up, preferred_element_type=jnp.float32)
    ).astype(jnp.bfloat16)
    row_block = dense_hidden
    dense_out = lax.psum_scatter(
        jnp.dot(row_block, dense_down, preferred_element_type=jnp.float32),
        "ep",
        scatter_dimension=0,
        tiled=True,
    )
    residual = lax.dynamic_slice_in_dim(mixed, tp_index * quarter_cols, quarter_cols, 1).astype(
        jnp.float32
    )
    return (residual + routed + gate_value[:, None] * dense_out).astype(jnp.bfloat16)


def solution(mesh):
    return jax.shard_map(
        shards,
        mesh=mesh,
        in_specs=(
            P("ep", None),
            P(),
            P("ep", "tp"),
            P("ep", "tp"),
            P("ep", "tp"),
            P("ep", "tp"),
            P("tp"),
            P("ep", None, "tp", None),
            P("ep", None, "tp"),
            P("ep"),
            P("tp", "ep"),
            P(),
            P("ep", None, "tp"),
            P("ep", None, "tp"),
            P("ep", "tp", None),
            P("ep", None),
            P("ep", None),
            P(None, "ep"),
            P(None, "ep"),
            P("ep", "tp"),
            P(),
        ),
        out_specs=P("ep", "tp"),
        check_vma=False,
    )
```

profile of v0, /device:TPU:0, one launch (start us, length us, event | category | flops | bytes accessed | tf_op | source)
XLA Modules:
  0.0 333.0 jit_solution(12179301577359732236)
XLA Ops:
  6.6 1.2 fusion.48
  8.9 14.4 %all_to_all.48 = bf16[16,8,512]{2,0,1:T(8,128)(2,1)S(1)} all-to-all(bf16[16,8,512]{2,0,1:T(8,128)(2,1)S(1)} %bitcast.121), channel_id=1, replica_groups=mesh['ep'=8,'tp'=4] {'ep'}, dimensions={1} | all-to-all | bytes 262144 | tf_op jit(solution)/shard_map/all_to_all | solution.py:84
  26.2 1.3 fusion.81
  29.4 59.1 %reduce-scatter.4.cloned.1.call-done = f32[16,648]{1,0:T(8,128)} async-done(((f32[128,648]{1,0:T(8,128)}), f32[16,648]{1,0:T(8,128)}) %reduce-scatter.4.cloned.1.call-update) | async-done | bytes 41488 | tf_op jit(solution)/shard_map/reduce_scatter | solution.py:86
  90.5 3.7 %fusion.80 = (f32[16,8]{1,0:T(8,128)S(1)}, f32[16,1,8,1024]{3,2,0,1:T(8,128)S(1)}) fusion(f32[16,1024,8]{1,2,0:T(8,128)S(1)} %copy-done.3, f32[16,8]{1,0:T(8,128)S(1)} %fusion.69, bf16[16,8,64]{2,1,0:T(8,128)(2,1)S(1)} %reshape.186, bf16[16,1024,1,128]{3,1,2,0:T(8,128)(2,1)} %param.28, pred[16,1024]{1,0:T(8,128)(4,1)S(1)} %iota_compare_fusion.1), kind=kOutput, calls=%fused_computation.96 | convolution fusion | flops 17432448 | bytes 5276672 | tf_op jit(solution)/shard_map/skgd,slkd->skgl/dot_general | solution.py:31
  94.5 1.4 fusion.37
  96.0 30.5 %all_gather.6 = bf16[128,512]{1,0:T(8,128)(2,1)S(1)} all-gather(bf16[16,512]{1,0:T(8,128)(2,1)S(1)} %reshape.191), channel_id=1, replica_groups=mesh['ep'=8,'tp'=4] {'ep'}, dimensions={0}, use_global_device_ids=true | all-gather | bytes 147456 | tf_op jit(solution)/shard_map/all_gather | solution.py:104
  127.7 31.3 %all-reduce.2.cloned.1.call-done = f32[8,16,512]{2,1,0:T(8,128)} async-done(((f32[8,16,512]{2,1,0:T(8,128)}), f32[8,16,512]{2,1,0:T(8,128)}) %all-reduce.2.cloned.1.call-update) | async-done | bytes 262160 | tf_op jit(solution)/shard_map/psum | solution.py:108
  159.0 5.5 %all-to-all-start.1 = ((f32[8,16,512]{2,1,0:T(8,128)}), f32[8,16,512]{2,1,0:T(8,128)S(1)}, u32[]{:S(2)}, u32[]{:S(2)}) async-start(f32[8,16,512]{2,1,0:T(8,128)} %all-reduce.2.cloned.1.call-done), calls=%async_computation.2 | async-start | bytes 524288 | tf_op jit(solution)/shard_map/all_to_all | solution.py:109
  165.2 7.6 %all-to-all-done.1 = f32[8,16,512]{2,1,0:T(8,128)S(1)} async-done(((f32[8,16,512]{2,1,0:T(8,128)}), f32[8,16,512]{2,1,0:T(8,128)S(1)}, u32[]{:S(2)}, u32[]{:S(2)}) %all-to-all-start.1) | async-done | bytes 262176 | tf_op jit(solution)/shard_map/all_to_all | solution.py:109
  173.1 1.5 convolution_convert_fusion
  174.6 3.6 %all-to-all-start.2 = ((bf16[8,16,4096]{2,1,0:T(8,128)(2,1)}), bf16[8,16,4096]{2,1,0:T(8,128)(2,1)S(1)}, u32[]{:S(2)}, u32[]{:S(2)}) async-start(bf16[8,16,4096]{2,1,0:T(8,128)(2,1)} %bitcast.112), calls=%async_computation.3 | async-start | bytes 2097152 | tf_op jit(solution)/shard_map/all_to_all | solution.py:132
  178.9 27.4 %all-to-all-done.2 = bf16[8,16,4096]{2,1,0:T(8,128)(2,1)S(1)} async-done(((bf16[8,16,4096]{2,1,0:T(8,128)(2,1)}), bf16[8,16,4096]{2,1,0:T(8,128)(2,1)S(1)}, u32[]{:S(2)}, u32[]{:S(2)}) %all-to-all-start.2) | async-done | bytes 1048608 | tf_op jit(solution)/shard_map/all_to_all | solution.py:132
  206.3 2.0 fusion.10
  208.4 4.3 %fusion.6 = f32[128,4096]{1,0:T(8,128)} fusion(bf16[1,256,4096]{2,1,0:T(8,128)(2,1)S(1)} %copy-done, bf16[128,4096]{1,0:T(8,128)(2,1)S(1)} %bitcast.110, bf16[1,4096,256]{2,1,0:T(8,128)(2,1)} %param.34, f32[128,256]{1,0:T(8,128)S(1)} %fusion.10), kind=kOutput, calls=%fused_computation.8 | convolution fusion | flops 537067520 | bytes 7471104 | tf_op jit(solution)/shard_map/dot_general | solution.py:138
  212.7 14.0 %all-gather.2.cloned.1.call-done = bf16[128,4096]{1,0:T(8,128)(2,1)} async-done(((bf16[16,4096]{1,0:T(8,128)(2,1)}), bf16[128,4096]{1,0:T(8,128)(2,1)}) %all-gather.2.cloned.1.call-update) | async-done | bytes 1048592 | tf_op jit(solution)/shard_map/all_gather | solution.py:150
  226.7 3.3 fusion.86
  230.1 4.3 %fusion.25 = f32[128,1024]{1,0:T(8,128)} fusion(bf16[512,1024]{1,0:T(8,128)(2,1)} %param.40, bf16[128,4096]{1,0:T(8,128)(2,1)S(1)} %copy-done.2, bf16[4096,512]{1,0:T(8,128)(2,1)} %param.39, f32[128,512]{1,0:T(8,128)S(1)} %fusion.86), kind=kOutput, calls=%fused_computation.20 | convolution fusion | flops 671481856 | bytes 7077888 | tf_op jit(solution)/shard_map/dot_general | solution.py:157
  234.6 24.5 %reduce-scatter.6.cloned.1.call-done = f32[128,1024]{1,0:T(8,128)} async-done(((f32[128,4096]{1,0:T(8,128)}), f32[128,1024]{1,0:T(8,128)}) %reduce-scatter.6.cloned.1.call-update) | async-done | bytes 524304 | tf_op jit(solution)/shard_map/reduce_scatter | solution.py:139
  259.0 1.8 convert_element_type.82
  260.8 5.5 %all-to-all-start.3 = ((bf16[8,16,1024]{2,1,0:T(8,128)(2,1)}), bf16[8,16,1024]{2,1,0:T(8,128)(2,1)S(1)}, u32[]{:S(2)}, u32[]{:S(2)}) async-start(bf16[8,16,1024]{2,1,0:T(8,128)(2,1)} %bitcast.19), calls=%async_computation.5 | async-start | bytes 524288 | tf_op jit(solution)/shard_map/all_to_all | solution.py:141
  267.3 8.6 %all-to-all-done.3 = bf16[8,16,1024]{2,1,0:T(8,128)(2,1)S(1)} async-done(((bf16[8,16,1024]{2,1,0:T(8,128)(2,1)}), bf16[8,16,1024]{2,1,0:T(8,128)(2,1)S(1)}, u32[]{:S(2)}, u32[]{:S(2)}) %all-to-all-start.3) | async-done | bytes 262176 | tf_op jit(solution)/shard_map/all_to_all | solution.py:141
  276.9 48.0 %reduce-scatter.8.cloned.1.call-done = f32[16,1024]{1,0:T(8,128)} async-done(((f32[128,1024]{1,0:T(8,128)}), f32[16,1024]{1,0:T(8,128)}) %reduce-scatter.8.cloned.1.call-update) | async-done | bytes 65552 | tf_op jit(solution)/shard_map/reduce_scatter | solution.py:156
  324.9 1.5 add_convert_fusion
  (81 shorter events, 13.2 us)
Async XLA Ops:
  6.5 201.8 %copy-start = (bf16[1,256,4096]{2,1,0:T(8,128)(2,1)S(1)}, bf16[1,256,4096]{2,1,0:T(8,128)(2,1)}, u32[]{:S(2)}) copy-start(bf16[1,256,4096]{2,1,0:T(8,128)(2,1)} %param.35) | copy-start | bytes 6291460
  6.5 22.8 %copy-start.12 = (s32[16]{0:T(128)S(1)}, s32[16]{0:T(128)}, u32[]{:S(2)}) copy-start(s32[16]{0:T(128)} %param.30) | copy-start | bytes 196
  6.5 22.6 %copy-start.3 = (f32[16,1024,8]{1,2,0:T(8,128)S(1)}, f32[16,1024,8]{1,2,0:T(8,128)}, u32[]{:S(2)}) copy-start(f32[16,1024,8]{1,2,0:T(8,128)} %param.29) | copy-start | bytes 1572868
  6.5 83.1 %copy-start.13 = (f32[8]{0:T(128)S(1)}, f32[8]{0:T(128)}, u32[]{:S(2)}) copy-start(f32[8]{0:T(128)} %param.27) | copy-start | bytes 100
  6.5 82.0 %reduce-scatter.4.cloned.1.call-start = ((), (), s32[]{:S(2)}) async-start(), calls=%async_computation.7 | async-start | bytes 442368 | tf_op jit(solution)/shard_map/reduce_scatter | solution.py:86
  28.3 130.7 %all-reduce.2.cloned.1.call-start = ((), (), s32[]{:S(2)}) async-start(), calls=%async_computation.8 | async-start | bytes 524288 | tf_op jit(solution)/shard_map/psum | solution.py:108
  89.5 5.0 %copy-start.1 = (bf16[16,1024,1,128]{3,1,2,0:T(8,128)(2,1)S(1)}, bf16[16,1024,1,128]{3,1,2,0:T(8,128)(2,1)}, u32[]{:S(2)}) copy-start(bf16[16,1024,1,128]{3,1,2,0:T(8,128)(2,1)} %param.28) | copy-start | bytes 12582916
  94.2 32.3 %copy-start.8 = (bf16[512,512]{1,0:T(8,128)(2,1)S(1)}, bf16[512,512]{1,0:T(8,128)(2,1)}, u32[]{:S(2)}) copy-start(bf16[512,512]{1,0:T(8,128)(2,1)} %param.31) | copy-start | bytes 1572868
  94.2 33.3 %copy-start.10 = (s32[16,4]{0,1:T(4,128)S(1)}, s32[16,4]{0,1:T(4,128)}, u32[]{:S(2)}) copy-start(s32[16,4]{0,1:T(4,128)} %param.36) | copy-start | bytes 772
  94.5 78.3 %copy-start.4 = (bf16[16,4096]{1,0:T(8,128)(2,1)S(1)}, bf16[16,4096]{1,0:T(8,128)(2,1)}, u32[]{:S(2)}) copy-start(bf16[16,4096]{1,0:T(8,128)(2,1)} %param.21) | copy-start | bytes 393220
  94.5 78.5 %copy-start.9 = (f32[4096]{0:T(1024)S(1)}, f32[4096]{0:T(1024)}, u32[]{:S(2)}) copy-start(f32[4096]{0:T(1024)} %param.32) | copy-start | bytes 49156
  159.0 13.7 %all-to-all-start.1 = ((f32[8,16,512]{2,1,0:T(8,128)}), f32[8,16,512]{2,1,0:T(8,128)S(1)}, u32[]{:S(2)}, u32[]{:S(2)}) async-start(f32[8,16,512]{2,1,0:T(8,128)} %all-reduce.2.cloned.1.call-done), calls=%async_computation.2 | async-start | bytes 524288 | tf_op jit(solution)/shard_map/all_to_all | solution.py:109
  173.0 1.6 copy-start.7
  173.1 5.1 %copy-start.5 = (bf16[16,4096]{1,0:T(8,128)(2,1)}, bf16[16,4096]{1,0:T(8,128)(2,1)S(1)}, u32[]{:S(2)}) copy-start(bf16[16,4096]{1,0:T(8,128)(2,1)S(1)} %fusion.47) | copy-start | bytes 393220
  174.6 31.8 %all-to-all-start.2 = ((bf16[8,16,4096]{2,1,0:T(8,128)(2,1)}), bf16[8,16,4096]{2,1,0:T(8,128)(2,1)S(1)}, u32[]{:S(2)}, u32[]{:S(2)}) async-start(bf16[8,16,4096]{2,1,0:T(8,128)(2,1)} %bitcast.112), calls=%async_computation.3 | async-start | bytes 2097152 | tf_op jit(solution)/shard_map/all_to_all | solution.py:132
  178.1 48.6 %all-gather.2.cloned.1.call-start = ((), (), s32[]{:S(2)}) async-start(), calls=%async_computation.10 | async-start | bytes 1179648 | tf_op jit(solution)/shard_map/all_gather | solution.py:150
  178.9 80.2 %reduce-scatter.6.cloned.1.call-start = ((), (), s32[]{:S(2)}) async-start(), calls=%async_computation.9 | async-start | bytes 2621440 | tf_op jit(solution)/shard_map/reduce_scatter | solution.py:139
  212.7 112.2 %reduce-scatter.8.cloned.1.call-start = ((), (), s32[]{:S(2)}) async-start(), calls=%async_computation.11 | async-start | bytes 589824 | tf_op jit(solution)/shard_map/reduce_scatter | solution.py:156
  226.7 3.3 copy-start.2
  230.1 4.3 %copy-start.11 = (f32[16,4]{0,1:T(4,128)S(1)}, f32[16,4]{0,1:T(4,128)}, u32[]{:S(2)}) copy-start(f32[16,4]{0,1:T(4,128)} %param.37) | copy-start | bytes 772
  230.1 36.3 %copy-start.6 = (bf16[16,4096]{1,0:T(8,128)(2,1)S(1)}, bf16[16,4096]{1,0:T(8,128)(2,1)}, u32[]{:S(2)}) copy-start(bf16[16,4096]{1,0:T(8,128)(2,1)} %copy-done.5) | copy-start | bytes 393220
  260.8 15.1 %all-to-all-start.3 = ((bf16[8,16,1024]{2,1,0:T(8,128)(2,1)}), bf16[8,16,1024]{2,1,0:T(8,128)(2,1)S(1)}, u32[]{:S(2)}, u32[]{:S(2)}) async-start(bf16[8,16,1024]{2,1,0:T(8,128)(2,1)} %bitcast.19), calls=%async_computation.5 | async-start | bytes 524288 | tf_op jit(solution)/shard_map/all_to_all | solution.py:141
Sparse Core Ops, SparseCore 0:
  28.5 60.0 reduce-scatter.3
  127.6 31.3 all-reduce.1
  181.1 45.6 all-gather.1
  229.1 29.8 reduce-scatter.5
  262.2 62.6 reduce-scatter.7
where the time goes:
time: 334 us; the launch traced here: 333 us
  waiting for transfers between devices  221 us (66%)
  blocking collectives  44.9 us (13%)
  matrix products  26.6 us (8%)
  starting transfers between devices  14.8 us (4%)
  between operations  13.5 us (4%)
  other arithmetic  10.4 us (3%)
    reduce_scatter x1, waiting for transfers between devices, shards(): lax.psum_scatter(jnp.concatenate([jnp.dot(row_block, matrix, preferred_el...  59.1 us
    reduce_scatter x1, waiting for transfers between devices, shards(): lax.psum_scatter(jnp.dot(row_block, dense_down, preferred_element_type=jn...  48 us
    psum x1, waiting for transfers between devices, shards(): column_total = lax.psum(column_terms, 'tp')  31.3 us
    all_gather x1, blocking collectives, shards(): lax.all_gather(attended, 'ep', axis=0, tiled=True)  30.5 us
    all_to_all x1, waiting for transfers between devices, shards(): lax.all_to_all(outgoing, 'ep', split_axis=0, concat_axis=0, tiled=True)  27.4 us
    reduce_scatter x1, waiting for transfers between devices, shards(): lax.psum_scatter(partial_rows, 'tp', scatter_dimension=1, tiled=True)  24.5 us
    all_to_all x1, blocking collectives, shards(): lax.all_to_all(normed, 'ep', split_axis=1, concat_axis=0, tiled=True)  14.4 us
    all_gather x1, waiting for transfers between devices, shards(): piece = lax.all_gather(second, 'ep', axis=0, tiled=True)  14 us
  transfers between devices with their start and end apart: 8, of which 8 were waited for; matrix products, arithmetic and copies ran while one was open for 6% of the time, Pallas kernels for 0%

commit v1 on v0

--- a/solution.py
+++ b/solution.py
@@ -105,7 +105,11 @@
         out_weight,
         preferred_element_type=jnp.float32,
     )
-    column_total = lax.psum(column_terms, "tp")
+    column_total = column_terms
+    for hop in (1, 2):
+        column_total = column_total + lax.ppermute(
+            column_total, "tp", [(dev, dev ^ hop) for dev in range(4)]
+        )
     summed = lax.all_to_all(column_total, "ep", split_axis=0, concat_axis=1, tiled=True)
     mixed = (tokens.astype(jnp.float32) + summed).astype(jnp.bfloat16)
     second = rms_scaled(mixed, mix_gain).astype(jnp.bfloat16)

time: 334 us -> 312 us (0.934)
  waiting for transfers between devices: 221 us -> 199 us
    psum x1 -> x0, waiting for transfers between devices: 31.3 us -> none  [shards(): column_total = lax.psum(column_terms, 'tp')]
    ppermute x0 -> x2, waiting for transfers between devices: none -> 8.23 us  [shards(): lax.ppermute(column_total, 'tp', [(dev, dev ^ hop) for dev in range(4)])]
  transfers between devices with their start and end apart: 8 -> 9, of which waited for: 8 -> 9; matrix products, arithmetic and copies ran while one was open for 6% -> 6% of each run, Pallas kernels for 0% -> 0%
where the time goes in v1:
time: 312 us; the launch traced here: 311 us
  waiting for transfers between devices  199 us (64%)
  blocking collectives  44.9 us (14%)
  matrix products  25.9 us (8%)
  starting transfers between devices  14.5 us (5%)
  between operations  13.4 us (4%)
  other arithmetic  11.2 us (4%)
    reduce_scatter x1, waiting for transfers between devices, shards(): lax.psum_scatter(jnp.concatenate([jnp.dot(row_block, matrix, preferred_el...  59.2 us
    reduce_scatter x1, waiting for transfers between devices, shards(): lax.psum_scatter(jnp.dot(row_block, dense_down, preferred_element_type=jn...  48 us
    all_gather x1, blocking collectives, shards(): lax.all_gather(attended, 'ep', axis=0, tiled=True)  30.5 us
    all_to_all x1, waiting for transfers between devices, shards(): lax.all_to_all(outgoing, 'ep', split_axis=0, concat_axis=0, tiled=True)  28.8 us
    reduce_scatter x1, waiting for transfers between devices, shards(): lax.psum_scatter(partial_rows, 'tp', scatter_dimension=1, tiled=True)  24.6 us
    all_to_all x1, blocking collectives, shards(): lax.all_to_all(normed, 'ep', split_axis=1, concat_axis=0, tiled=True)  14.4 us
    all_gather x1, waiting for transfers between devices, shards(): piece = lax.all_gather(second, 'ep', axis=0, tiled=True)  13.3 us
    all_to_all x1, waiting for transfers between devices, shards(): lax.all_to_all(replies, 'ep', split_axis=0, concat_axis=0, tiled=True)  8.57 us
  transfers between devices with their start and end apart: 9, of which 9 were waited for; matrix products, arithmetic and copies ran while one was open for 6% of the time, Pallas kernels for 0%

profile of v1, /device:TPU:0, one launch (start us, length us, event | category | flops | bytes accessed | tf_op | source)
XLA Modules:
  0.0 310.9 jit_solution(5733466003041281708)
XLA Ops:
  8.9 14.4 %all_to_all.48 = bf16[16,8,512]{2,0,1:T(8,128)(2,1)S(1)} all-to-all(bf16[16,8,512]{2,0,1:T(8,128)(2,1)S(1)} %bitcast.120), channel_id=1, replica_groups=mesh['ep'=8,'tp'=4] {'ep'}, dimensions={1} | all-to-all | bytes 262144 | tf_op jit(solution)/shard_map/all_to_all | solution.py:84
  29.4 59.2 %reduce-scatter.4.cloned.1.call-done = f32[16,648]{1,0:T(8,128)} async-done(((f32[128,648]{1,0:T(8,128)}), f32[16,648]{1,0:T(8,128)}) %reduce-scatter.4.cloned.1.call-update) | async-done | bytes 41488 | tf_op jit(solution)/shard_map/reduce_scatter | solution.py:86
  90.5 3.7 %fusion.80 = (f32[16,8]{1,0:T(8,128)S(1)}, f32[16,1,8,1024]{3,2,0,1:T(8,128)S(1)}) fusion(f32[16,1024,8]{1,2,0:T(8,128)S(1)} %copy-done.3, f32[16,8]{1,0:T(8,128)S(1)} %fusion.69, bf16[16,8,64]{2,1,0:T(8,128)(2,1)S(1)} %reshape.186, bf16[16,1024,1,128]{3,1,2,0:T(8,128)(2,1)} %param.28, pred[16,1024]{1,0:T(8,128)(4,1)S(1)} %iota_compare_fusion.1), kind=kOutput, calls=%fused_computation.96 | convolution fusion | flops 17432448 | bytes 5276672 | tf_op jit(solution)/shard_map/skgd,slkd->skgl/dot_general | solution.py:31
  94.6 1.4 fusion.37
  96.1 30.5 %all_gather.6 = bf16[128,512]{1,0:T(8,128)(2,1)S(1)} all-gather(bf16[16,512]{1,0:T(8,128)(2,1)S(1)} %reshape.191), channel_id=1, replica_groups=mesh['ep'=8,'tp'=4] {'ep'}, dimensions={0}, use_global_device_ids=true | all-gather | bytes 147456 | tf_op jit(solution)/shard_map/all_gather | solution.py:104
  126.9 1.5 collective-permute-done
  128.5 1.5 collective-permute-start.1
  130.2 6.7 %collective-permute-done.1 = f32[128,512]{1,0:T(8,128)S(1)} collective-permute-done((f32[128,512]{1,0:T(8,128)S(1)}, f32[128,512]{1,0:T(8,128)S(1)}, u32[]{:S(2)}, u32[]{:S(2)}) %collective-permute-start.1) | collective-permute-done | bytes 262176 | tf_op jit(solution)/shard_map/ppermute | solution.py:110
  137.6 3.7 %all-to-all-start.1 = ((f32[8,16,512]{2,1,0:T(8,128)}), f32[8,16,512]{2,1,0:T(8,128)S(1)}, u32[]{:S(2)}, u32[]{:S(2)}) async-start(f32[8,16,512]{2,1,0:T(8,128)} %bitcast.12), calls=%async_computation.2 | async-start | bytes 524288 | tf_op jit(solution)/shard_map/all_to_all | solution.py:113
  141.9 7.9 %all-to-all-done.1 = f32[8,16,512]{2,1,0:T(8,128)S(1)} async-done(((f32[8,16,512]{2,1,0:T(8,128)}), f32[8,16,512]{2,1,0:T(8,128)S(1)}, u32[]{:S(2)}, u32[]{:S(2)}) %all-to-all-start.1) | async-done | bytes 262176 | tf_op jit(solution)/shard_map/all_to_all | solution.py:113
  150.1 1.5 convolution_convert_fusion
  151.6 3.6 %all-to-all-start.2 = ((bf16[8,16,4096]{2,1,0:T(8,128)(2,1)}), bf16[8,16,4096]{2,1,0:T(8,128)(2,1)S(1)}, u32[]{:S(2)}, u32[]{:S(2)}) async-start(bf16[8,16,4096]{2,1,0:T(8,128)(2,1)} %bitcast.112), calls=%async_computation.3 | async-start | bytes 2097152 | tf_op jit(solution)/shard_map/all_to_all | solution.py:136
  155.9 28.8 %all-to-all-done.2 = bf16[8,16,4096]{2,1,0:T(8,128)(2,1)S(1)} async-done(((bf16[8,16,4096]{2,1,0:T(8,128)(2,1)}), bf16[8,16,4096]{2,1,0:T(8,128)(2,1)S(1)}, u32[]{:S(2)}, u32[]{:S(2)}) %all-to-all-start.2) | async-done | bytes 1048608 | tf_op jit(solution)/shard_map/all_to_all | solution.py:136
  184.8 2.0 fusion.10
  186.8 4.2 %fusion.6 = f32[128,4096]{1,0:T(8,128)} fusion(bf16[1,256,4096]{2,1,0:T(8,128)(2,1)S(1)} %copy-done, bf16[128,4096]{1,0:T(8,128)(2,1)S(1)} %bitcast.110, bf16[1,4096,256]{2,1,0:T(8,128)(2,1)} %param.34, f32[128,256]{1,0:T(8,128)S(1)} %fusion.10), kind=kOutput, calls=%fused_computation.8 | convolution fusion | flops 537067520 | bytes 7471104 | tf_op jit(solution)/shard_map/dot_general | solution.py:142
  191.1 13.3 %all-gather.2.cloned.1.call-done = bf16[128,4096]{1,0:T(8,128)(2,1)} async-done(((bf16[16,4096]{1,0:T(8,128)(2,1)}), bf16[128,4096]{1,0:T(8,128)(2,1)}) %all-gather.2.cloned.1.call-update) | async-done | bytes 1048592 | tf_op jit(solution)/shard_map/all_gather | solution.py:154
  204.5 3.3 %fusion.86 = f32[128,512]{1,0:T(8,128)S(1)} fusion(bf16[128,4096]{1,0:T(8,128)(2,1)} %all-gather.2.cloned.1.call-done, bf16[4096,512]{1,0:T(8,128)(2,1)} %param.38), kind=kOutput, calls=%fused_computation.102 | convolution fusion | flops 536870912 | bytes 5505024 | tf_op jit(solution)/shard_map/dot_general | solution.py:156
  207.8 4.3 %fusion.25 = f32[128,1024]{1,0:T(8,128)} fusion(bf16[512,1024]{1,0:T(8,128)(2,1)} %param.40, bf16[128,4096]{1,0:T(8,128)(2,1)S(1)} %copy-done.2, bf16[4096,512]{1,0:T(8,128)(2,1)} %param.39, f32[128,512]{1,0:T(8,128)S(1)} %fusion.86), kind=kOutput, calls=%fused_computation.20 | convolution fusion | flops 671481856 | bytes 7077888 | tf_op jit(solution)/shard_map/dot_general | solution.py:161
  212.3 24.6 %reduce-scatter.6.cloned.1.call-done = f32[128,1024]{1,0:T(8,128)} async-done(((f32[128,4096]{1,0:T(8,128)}), f32[128,1024]{1,0:T(8,128)}) %reduce-scatter.6.cloned.1.call-update) | async-done | bytes 524304 | tf_op jit(solution)/shard_map/reduce_scatter | solution.py:143
  236.9 1.8 convert_element_type.82
  238.7 5.5 %all-to-all-start.3 = ((bf16[8,16,1024]{2,1,0:T(8,128)(2,1)}), bf16[8,16,1024]{2,1,0:T(8,128)(2,1)S(1)}, u32[]{:S(2)}, u32[]{:S(2)}) async-start(bf16[8,16,1024]{2,1,0:T(8,128)(2,1)} %bitcast.19), calls=%async_computation.5 | async-start | bytes 524288 | tf_op jit(solution)/shard_map/all_to_all | solution.py:145
  245.2 8.6 %all-to-all-done.3 = bf16[8,16,1024]{2,1,0:T(8,128)(2,1)S(1)} async-done(((bf16[8,16,1024]{2,1,0:T(8,128)(2,1)}), bf16[8,16,1024]{2,1,0:T(8,128)(2,1)S(1)}, u32[]{:S(2)}, u32[]{:S(2)}) %all-to-all-start.3) | async-done | bytes 262176 | tf_op jit(solution)/shard_map/all_to_all | solution.py:145
  254.8 48.0 %reduce-scatter.8.cloned.1.call-done = f32[16,1024]{1,0:T(8,128)} async-done(((f32[128,1024]{1,0:T(8,128)}), f32[16,1024]{1,0:T(8,128)}) %reduce-scatter.8.cloned.1.call-update) | async-done | bytes 65552 | tf_op jit(solution)/shard_map/reduce_scatter | solution.py:160
  302.8 1.5 add_convert_fusion
  (84 shorter events, 15.8 us)
Async XLA Ops:
  6.5 180.3 %copy-start = (bf16[1,256,4096]{2,1,0:T(8,128)(2,1)S(1)}, bf16[1,256,4096]{2,1,0:T(8,128)(2,1)}, u32[]{:S(2)}) copy-start(bf16[1,256,4096]{2,1,0:T(8,128)(2,1)} %param.35) | copy-start | bytes 6291460
  6.5 22.7 %copy-start.12 = (s32[16]{0:T(128)S(1)}, s32[16]{0:T(128)}, u32[]{:S(2)}) copy-start(s32[16]{0:T(128)} %param.30) | copy-start | bytes 196
  6.5 22.6 %copy-start.3 = (f32[16,1024,8]{1,2,0:T(8,128)S(1)}, f32[16,1024,8]{1,2,0:T(8,128)}, u32[]{:S(2)}) copy-start(f32[16,1024,8]{1,2,0:T(8,128)} %param.29) | copy-start | bytes 1572868
  6.5 83.1 %copy-start.13 = (f32[8]{0:T(128)S(1)}, f32[8]{0:T(128)}, u32[]{:S(2)}) copy-start(f32[8]{0:T(128)} %param.27) | copy-start | bytes 100
  6.5 82.0 %reduce-scatter.4.cloned.1.call-start = ((), (), s32[]{:S(2)}) async-start(), calls=%async_computation.7 | async-start | bytes 442368 | tf_op jit(solution)/shard_map/reduce_scatter | solution.py:86
  89.5 5.0 %copy-start.1 = (bf16[16,1024,1,128]{3,1,2,0:T(8,128)(2,1)S(1)}, bf16[16,1024,1,128]{3,1,2,0:T(8,128)(2,1)}, u32[]{:S(2)}) copy-start(bf16[16,1024,1,128]{3,1,2,0:T(8,128)(2,1)} %param.28) | copy-start | bytes 12582916
  94.2 32.3 %copy-start.8 = (bf16[512,512]{1,0:T(8,128)(2,1)S(1)}, bf16[512,512]{1,0:T(8,128)(2,1)}, u32[]{:S(2)}) copy-start(bf16[512,512]{1,0:T(8,128)(2,1)} %param.31) | copy-start | bytes 1572868
  94.5 35.5 %copy-start.10 = (s32[16,4]{0,1:T(4,128)S(1)}, s32[16,4]{0,1:T(4,128)}, u32[]{:S(2)}) copy-start(s32[16,4]{0,1:T(4,128)} %param.36) | copy-start | bytes 772
  94.5 55.3 %copy-start.4 = (bf16[16,4096]{1,0:T(8,128)(2,1)S(1)}, bf16[16,4096]{1,0:T(8,128)(2,1)}, u32[]{:S(2)}) copy-start(bf16[16,4096]{1,0:T(8,128)(2,1)} %param.21) | copy-start | bytes 393220
  94.5 55.5 %copy-start.9 = (f32[4096]{0:T(1024)S(1)}, f32[4096]{0:T(1024)}, u32[]{:S(2)}) copy-start(f32[4096]{0:T(1024)} %param.32) | copy-start | bytes 49156
  126.8 1.6 collective-permute-start
  128.5 8.4 %collective-permute-start.1 = (f32[128,512]{1,0:T(8,128)S(1)}, f32[128,512]{1,0:T(8,128)S(1)}, u32[]{:S(2)}, u32[]{:S(2)}) collective-permute-start(f32[128,512]{1,0:T(8,128)S(1)} %add.115), channel_id=1, source_target_pairs={{0,2},{1,3},{2,0},{3,1},{4,6},{5,7},{6,4},{7,5},{8,10},{9,11},{10,... | collective-permute-start | bytes 786440 | tf_op jit(solution)/shard_map/ppermute | solution.py:110
  137.6 12.2 %all-to-all-start.1 = ((f32[8,16,512]{2,1,0:T(8,128)}), f32[8,16,512]{2,1,0:T(8,128)S(1)}, u32[]{:S(2)}, u32[]{:S(2)}) async-start(f32[8,16,512]{2,1,0:T(8,128)} %bitcast.12), calls=%async_computation.2 | async-start | bytes 524288 | tf_op jit(solution)/shard_map/all_to_all | solution.py:113
  150.0 1.6 copy-start.7
  150.1 5.1 %copy-start.5 = (bf16[16,4096]{1,0:T(8,128)(2,1)}, bf16[16,4096]{1,0:T(8,128)(2,1)S(1)}, u32[]{:S(2)}) copy-start(bf16[16,4096]{1,0:T(8,128)(2,1)S(1)} %fusion.47) | copy-start | bytes 393220
  151.6 33.2 %all-to-all-start.2 = ((bf16[8,16,4096]{2,1,0:T(8,128)(2,1)}), bf16[8,16,4096]{2,1,0:T(8,128)(2,1)S(1)}, u32[]{:S(2)}, u32[]{:S(2)}) async-start(bf16[8,16,4096]{2,1,0:T(8,128)(2,1)} %bitcast.112), calls=%async_computation.3 | async-start | bytes 2097152 | tf_op jit(solution)/shard_map/all_to_all | solution.py:136
  155.1 49.3 %all-gather.2.cloned.1.call-start = ((), (), s32[]{:S(2)}) async-start(), calls=%async_computation.9 | async-start | bytes 1179648 | tf_op jit(solution)/shard_map/all_gather | solution.py:154
  155.9 81.0 %reduce-scatter.6.cloned.1.call-start = ((), (), s32[]{:S(2)}) async-start(), calls=%async_computation.8 | async-start | bytes 2621440 | tf_op jit(solution)/shard_map/reduce_scatter | solution.py:143
  191.1 111.7 %reduce-scatter.8.cloned.1.call-start = ((), (), s32[]{:S(2)}) async-start(), calls=%async_computation.10 | async-start | bytes 589824 | tf_op jit(solution)/shard_map/reduce_scatter | solution.py:160
  204.5 3.3 %copy-start.2 = (bf16[128,4096]{1,0:T(8,128)(2,1)S(1)}, bf16[128,4096]{1,0:T(8,128)(2,1)}, u32[]{:S(2)}) copy-start(bf16[128,4096]{1,0:T(8,128)(2,1)} %all-gather.2.cloned.1.call-done) | copy-start | bytes 3145732
  207.8 4.3 %copy-start.11 = (f32[16,4]{0,1:T(4,128)S(1)}, f32[16,4]{0,1:T(4,128)}, u32[]{:S(2)}) copy-start(f32[16,4]{0,1:T(4,128)} %param.37) | copy-start | bytes 772
  207.8 36.4 %copy-start.6 = (bf16[16,4096]{1,0:T(8,128)(2,1)S(1)}, bf16[16,4096]{1,0:T(8,128)(2,1)}, u32[]{:S(2)}) copy-start(bf16[16,4096]{1,0:T(8,128)(2,1)} %copy-done.5) | copy-start | bytes 393220
  238.7 15.1 %all-to-all-start.3 = ((bf16[8,16,1024]{2,1,0:T(8,128)(2,1)}), bf16[8,16,1024]{2,1,0:T(8,128)(2,1)S(1)}, u32[]{:S(2)}, u32[]{:S(2)}) async-start(bf16[8,16,1024]{2,1,0:T(8,128)(2,1)} %bitcast.19), calls=%async_computation.5 | async-start | bytes 524288 | tf_op jit(solution)/shard_map/all_to_all | solution.py:145
Sparse Core Ops, SparseCore 0:
  28.5 60.0 reduce-scatter.3
  158.1 46.3 all-gather.1
  207.0 29.8 reduce-scatter.5
  240.1 62.6 reduce-scatter.7
